TPU v7x, 32 devices: a whole 2x2x4 slice. The times are simulated.
32 devices in a mesh: sp: 8 (over z, y), tp: 4 (over x, core).
Axes of the slice: x: 2, y: 2, z: 4, core: 2. Of those that a mesh axis runs over, the one named last changes fastest.
Arguments:
- stream: bfloat16 [4096, 2048], P('sp', 'tp'), may hold values from -6 to 6
- doc_ids: int32 [4096], P('sp'), may hold values from 0 to 3, never falling along the last dimension, each value on 1 to 2304 neighbouring positions
- norm_gain: float32 [2, 2048], replicated, may hold values from 0.1 to 1.9
- gate_proj: bfloat16 [2, 2048, 2048], P(None, 'sp', 'tp'), may hold values from -0.125 to 0.125
- input_gate: bfloat16 [2, 2048, 2048], P(None, 'sp', 'tp'), may hold values from -0.125 to 0.125
- value_proj: bfloat16 [2, 2048, 2048], P(None, 'sp', 'tp'), may hold values from -0.125 to 0.125
- taps: float32 [2, 3, 2048], P(None, None, 'tp'), may hold values from -3 to 3
- out_proj: bfloat16 [2, 2048, 2048], P(None, 'tp', 'sp'), may hold values from -0.125 to 0.125
Outputs:
- result: bfloat16 [4096, 2048], P('sp', 'tp')
Inputs may be any that keep to these rules, and one draw needn't show every extreme that they name: `doc_ids`: document numbers never fall along the sequence; each document holds 1 to 2304 positions.
All inputs are finite; a program needn't handle non-finite values.
Results may differ from a plain program's by a relative error of at most 0.03.
Values may be sent and summed in bfloat16 or wider, within the bound.
A program may use at most 64 MiB of HBM per device.

v0:
```python
import jax
import jax.numpy as jnp
from jax import lax
from jax.sharding import PartitionSpec as P

epsilon = 1e-06


def with_halo(value, sides, width):
    for axis, dim in sides:
        size, length = (lax.axis_size(axis), value.shape[dim])
        up = [(i, (i + 1) % size) for i in range(size - 1)]
        down = [(j, i) for i, j in up]
        last = lax.slice_in_dim(value, length - width, length, axis=dim)
        leading = lax.slice_in_dim(value, 0, width, axis=dim)
        before = lax.ppermute(last, axis, up)
        after = lax.ppermute(leading, axis, down)
        value = jnp.concatenate([before, value, after], axis=dim)
    return value


def per_device(stream, doc_ids, norm_gain, gate_proj, input_gate, value_proj, taps, out_proj):
    layers = gate_proj.shape[0]
    gathered_in = (
        lax.all_gather(gate_proj, "sp", axis=1, tiled=True),
        lax.all_gather(input_gate, "sp", axis=1, tiled=True),
        lax.all_gather(value_proj, "sp", axis=1, tiled=True),
    )
    gathered_out = lax.all_gather(out_proj, "sp", axis=2, tiled=True)
    current = stream
    for layer_index in range(layers):
        full_rows = lax.all_gather(current, "tp", axis=1, tiled=True)
        widened = full_rows.astype(jnp.float32)
        scale = lax.rsqrt(jnp.mean(widened * widened, axis=-1, keepdims=True) + epsilon)
        normed = (widened * scale * norm_gain[layer_index]).astype(jnp.bfloat16)
        gate_b = jnp.dot(normed, gathered_in[0][layer_index], preferred_element_type=jnp.float32)
        gate_c = jnp.dot(normed, gathered_in[1][layer_index], preferred_element_type=jnp.float32)
        values = jnp.dot(normed, gathered_in[2][layer_index], preferred_element_type=jnp.float32)
        gate_b = gate_b.astype(jnp.bfloat16)
        gate_c = gate_c.astype(jnp.bfloat16)
        values = values.astype(jnp.bfloat16)
        mixed_in = (gate_c.astype(jnp.float32) * values.astype(jnp.float32)).astype(jnp.bfloat16)
        padded, doc_padded = (
            with_halo(mixed_in, (("sp", 0),), 1),
            with_halo(doc_ids, (("sp", 0),), 1),
        )
        same_prev = (doc_padded[:-2] == doc_ids)[:, None]
        same_next = (doc_padded[2:] == doc_ids)[:, None]
        kernel_taps = taps[layer_index]
        convolved = (
            jnp.where(same_prev, kernel_taps[0] * padded[:-2].astype(jnp.float32), 0.0)
            + kernel_taps[1] * mixed_in.astype(jnp.float32)
            + jnp.where(same_next, kernel_taps[2] * padded[2:].astype(jnp.float32), 0.0)
        )
        gated = (gate_b.astype(jnp.float32) * convolved).astype(jnp.bfloat16)
        partials = jnp.dot(gated, gathered_out[layer_index], preferred_element_type=jnp.float32)
        summed = lax.psum_scatter(
            partials.astype(jnp.bfloat16), "tp", scatter_dimension=1, tiled=True
        ).astype(jnp.float32)
        current = (current.astype(jnp.float32) + summed).astype(jnp.bfloat16)
    return current


def solution(mesh):
    in_specs = (
        P("sp", "tp"),
        P("sp"),
        P(),
        P(None, "sp", "tp"),
        P(None, "sp", "tp"),
        P(None, "sp", "tp"),
        P(None, None, "tp"),
        P(None, "tp", "sp"),
    )
    out_specs = P("sp", "tp")
    return jax.shard_map(
        per_device, mesh=mesh, in_specs=in_specs, out_specs=out_specs, check_vma=False
    )
```

profile of v0, /device:TPU:0, one launch (start us, length us, event | category | flops | bytes accessed | tf_op | source)
XLA Modules:
  0.0 454.6 jit_solution(15519410524372381653)
XLA Ops:
  6.5 0.0 all-gather.7.cloned.1.call-start
  6.5 0.7 all-gather.7.cloned.1.call-update
  7.3 0.0 all-gather.13.cloned.1.call-start
  7.3 0.7 all-gather.13.cloned.1.call-update
  8.0 0.0 all-gather.11.cloned.1.call-start
  8.1 0.7 all-gather.11.cloned.1.call-update
  8.7 0.0 all-gather.9.cloned.1.call-start
  8.8 0.5 all-gather.9.cloned.1.call-update
  9.3 0.0 all-gather.15.cloned.1.call-start
  9.4 0.5 all-gather.15.cloned.1.call-update
  9.9 0.0 reduce-scatter.3.cloned.1.call-start
  9.9 1.3 fusion.64
  11.3 5.4 %collective-permute-start = (s32[1]{0:T(128)}, s32[1]{0:T(128)}, u32[]{:S(2)}, u32[]{:S(2)}) collective-permute-start(s32[1]{0:T(128)} %get-tuple-element.21), channel_id=1, source_target_pairs={{0,4},{4,8},{8,12},{12,16},{16,20},{20,24},{24,28},{1,5},{5,9},{9,... | collective-permute-start | bytes 20 | tf_op jit(solution)/shard_map/ppermute | solution.py:16
  16.7 1.3 collective-permute-start.2
  18.0 0.8 fusion.63
  18.8 0.8 fusion.62
  19.6 0.0 collective-permute-done
  19.6 2.5 collective-permute-done.2
  22.2 2.1 pad_add_fusion
  24.3 9.9 %all-gather.7.cloned.1.call-done = bf16[512,2048]{1,0:T(8,128)(2,1)} async-done(((bf16[512,512]{1,0:T(8,128)(2,1)}), bf16[512,2048]{1,0:T(8,128)(2,1)}) %all-gather.7.cloned.1.call-update) | async-done | bytes 2097168 | tf_op jit(solution)/shard_map/all_gather | solution.py:32
  34.2 2.1 fusion
  36.3 72.9 %all-gather.13.cloned.1.call-done = bf16[2,2048,512]{2,1,0:T(8,128)(2,1)} async-done(((bf16[2,256,512]{2,1,0:T(8,128)(2,1)}), bf16[2,2048,512]{2,1,0:T(8,128)(2,1)}) %all-gather.13.cloned.1.call-update) | async-done | bytes 4194320 | tf_op jit(solution)/shard_map/all_gather | solution.py:27
  109.2 0.0 copy-start.2
  109.2 4.7 %fusion.19 = f32[512,512]{1,0:T(8,128)} fusion(bf16[2,2048,512]{2,1,0:T(8,128)(2,1)} %all-gather.13.cloned.1.call-done, bf16[512,2048]{1,0:T(8,128)(2,1)} %all-gather.7.cloned.1.call-done, f32[2048]{0:T(1024)S(1)} %bitcast.79, f32[512]{0:T(512)S(1)} %add_rsqrt_fusion.1), kind=kOutput, calls=%fused_computation.33 | convolution fusion | flops 1078460416 | bytes 5253120 | tf_op jit(solution)/shard_map/dot_general | solution.py:38
  113.9 0.0 copy-start.4
  113.9 68.9 %all-gather.11.cloned.1.call-done = bf16[2,2048,512]{2,1,0:T(8,128)(2,1)} async-done(((bf16[2,256,512]{2,1,0:T(8,128)(2,1)}), bf16[2,2048,512]{2,1,0:T(8,128)(2,1)}) %all-gather.11.cloned.1.call-update) | async-done | bytes 4194320 | tf_op jit(solution)/shard_map/all_gather | solution.py:26
  182.7 0.0 copy-done.2
  182.7 3.1 fusion.30
  185.9 2.5 collective-permute-start.1
  188.4 1.3 collective-permute-start.3
  189.7 0.0 copy-done.4
  189.7 0.1 slice_compare_fusion.1
  189.8 66.4 %all-gather.9.cloned.1.call-done = bf16[2,2048,512]{2,1,0:T(8,128)(2,1)} async-done(((bf16[2,256,512]{2,1,0:T(8,128)(2,1)}), bf16[2,2048,512]{2,1,0:T(8,128)(2,1)}) %all-gather.9.cloned.1.call-update) | async-done | bytes 4194320 | tf_op jit(solution)/shard_map/all_gather | solution.py:25
  256.1 75.1 %all-gather.15.cloned.1.call-done = bf16[2,512,2048]{2,1,0:T(8,128)(2,1)} async-done(((bf16[2,512,256]{2,1,0:T(8,128)(2,1)}), bf16[2,512,2048]{2,1,0:T(8,128)(2,1)}) %all-gather.15.cloned.1.call-update) | async-done | bytes 4194320 | tf_op jit(solution)/shard_map/all_gather | solution.py:29
  331.2 0.0 collective-permute-done.1
  331.2 0.0 collective-permute-done.3
  331.2 0.0 copy-start.1
  331.2 6.3 %convolution_convert_fusion.1 = bf16[512,2048]{1,0:T(8,128)(2,1)} fusion(bf16[2,512,2048]{2,1,0:T(8,128)(2,1)} %all-gather.15.cloned.1.call-done, bf16[2,2048,512]{2,1,0:T(8,128)(2,1)} %all-gather.9.cloned.1.call-done, bf16[512,512]{1,0:T(8,128)(2,1)S(1)} %fusion.30, bf16[1,512]{1,0:T(2,128)(2,1)S(1)} %collective-permute-done.3, ...), kind=kOutput, calls=%fused_computation.11 | convolution fusion | flops 2157969408 | bytes 8932352 | tf_op jit(solution)/shard_map/dot_general | solution.py:56
  337.5 0.0 reduce-scatter.3.cloned.1.call-update
  337.6 0.0 all-gather.17.cloned.1.call-start
  337.6 29.4 %reduce-scatter.3.cloned.1.call-done = bf16[512,512]{1,0:T(8,128)(2,1)} async-done(((bf16[512,2048]{1,0:T(8,128)(2,1)}), bf16[512,512]{1,0:T(8,128)(2,1)}) %reduce-scatter.3.cloned.1.call-update) | async-done | bytes 524304 | tf_op jit(solution)/shard_map/reduce_scatter | solution.py:57
  367.0 0.0 copy-done.1
  367.1 2.0 add_convert_fusion.1
  369.0 0.0 all-gather.17.cloned.1.call-update
  369.0 0.0 reduce-scatter.5.cloned.1.call-start
  369.1 22.7 %all-gather.17.cloned.1.call-done = bf16[512,2048]{1,0:T(8,128)(2,1)} async-done(((bf16[512,512]{1,0:T(8,128)(2,1)}), bf16[512,2048]{1,0:T(8,128)(2,1)}) %all-gather.17.cloned.1.call-update) | async-done | bytes 2097168 | tf_op jit(solution)/shard_map/all_gather | solution.py:32
  391.8 2.1 fusion.3
  393.8 0.0 copy-start.3
  393.8 0.0 copy-start.5
  393.9 3.7 fusion.27
  397.5 0.0 copy-done.3
  397.5 0.4 copy-done.5
  397.9 1.3 fusion.28
  399.2 3.4 collective-permute-start.4
  402.6 1.3 collective-permute-start.5
  403.9 0.0 collective-permute-done.4
  403.9 4.2 collective-permute-done.5
  408.1 0.0 copy-start
  408.1 6.3 %convolution_convert_fusion = bf16[512,2048]{1,0:T(8,128)(2,1)} fusion(bf16[2,512,2048]{2,1,0:T(8,128)(2,1)} %all-gather.15.cloned.1.call-done, bf16[2,2048,512]{2,1,0:T(8,128)(2,1)} %all-gather.9.cloned.1.call-done, bf16[512,512]{1,0:T(8,128)(2,1)S(1)} %fusion.28, bf16[1,512]{1,0:T(2,128)(2,1)S(1)} %collective-permute-done.5, ...), kind=kOutput, calls=%fused_computation.10 | convolution fusion | flops 2157969408 | bytes 8932352 | tf_op jit(solution)/shard_map/dot_general | solution.py:56
  414.4 0.0 reduce-scatter.5.cloned.1.call-update
  414.5 31.3 %reduce-scatter.5.cloned.1.call-done = bf16[512,512]{1,0:T(8,128)(2,1)} async-done(((bf16[512,2048]{1,0:T(8,128)(2,1)}), bf16[512,512]{1,0:T(8,128)(2,1)}) %reduce-scatter.5.cloned.1.call-update) | async-done | bytes 524304 | tf_op jit(solution)/shard_map/reduce_scatter | solution.py:57
  445.8 0.0 copy-done
  445.8 2.0 add_convert_fusion
  (4 shorter events, 0.0 us)
Async XLA Ops:
  6.5 27.7 %all-gather.7.cloned.1.call-start = ((), (), s32[]{:S(2)}) async-start(), calls=%async_computation.2 | async-start | bytes 2621440 | tf_op jit(solution)/shard_map/all_gather | solution.py:32
  7.3 101.9 %all-gather.13.cloned.1.call-start = ((), (), s32[]{:S(2)}) async-start(), calls=%async_computation.5 | async-start | bytes 4718592 | tf_op jit(solution)/shard_map/all_gather | solution.py:27
  8.0 174.7 %all-gather.11.cloned.1.call-start = ((), (), s32[]{:S(2)}) async-start(), calls=%async_computation.4 | async-start | bytes 4718592 | tf_op jit(solution)/shard_map/all_gather | solution.py:26
  8.7 247.4 %all-gather.9.cloned.1.call-start = ((), (), s32[]{:S(2)}) async-start(), calls=%async_computation.3 | async-start | bytes 4718592 | tf_op jit(solution)/shard_map/all_gather | solution.py:25
  9.3 321.9 %all-gather.15.cloned.1.call-start = ((), (), s32[]{:S(2)}) async-start(), calls=%async_computation.6 | async-start | bytes 4718592 | tf_op jit(solution)/shard_map/all_gather | solution.py:29
  9.9 357.1 %reduce-scatter.3.cloned.1.call-start = ((), (), s32[]{:S(2)}) async-start(), calls=%async_computation.7 | async-start | bytes 2621440 | tf_op jit(solution)/shard_map/reduce_scatter | solution.py:57
  11.3 8.3 %collective-permute-start = (s32[1]{0:T(128)}, s32[1]{0:T(128)}, u32[]{:S(2)}, u32[]{:S(2)}) collective-permute-start(s32[1]{0:T(128)} %get-tuple-element.21), channel_id=1, source_target_pairs={{0,4},{4,8},{8,12},{12,16},{16,20},{20,24},{24,28},{1,5},{5,9},{9,... | collective-permute-start | bytes 20 | tf_op jit(solution)/shard_map/ppermute | solution.py:16
  16.7 5.5 %collective-permute-start.2 = (s32[1]{0:T(128)}, s32[1]{0:T(128)}, u32[]{:S(2)}, u32[]{:S(2)}) collective-permute-start(s32[1]{0:T(128)} %get-tuple-element.22), channel_id=1, source_target_pairs={{4,0},{8,4},{12,8},{16,12},{20,16},{24,20},{28,24},{5,1},{9,5},{13... | collective-permute-start | bytes 20 | tf_op jit(solution)/shard_map/ppermute | solution.py:17
  109.2 73.5 %copy-start.2 = (bf16[512,2048]{1,0:T(8,128)(2,1)S(1)}, bf16[512,2048]{1,0:T(8,128)(2,1)}, u32[]{:S(2)}) copy-start(bf16[512,2048]{1,0:T(8,128)(2,1)} %all-gather.7.cloned.1.call-done) | copy-start | bytes 6291460
  113.9 75.8 %copy-start.4 = (s32[512]{0:T(512)S(1)}, s32[512]{0:T(512)}, u32[]{:S(2)}) copy-start(s32[512]{0:T(512)} %param.9) | copy-start | bytes 6148
  185.9 145.3 %collective-permute-start.1 = (bf16[1,512]{1,0:T(2,128)(2,1)S(1)}, bf16[1,512]{1,0:T(2,128)(2,1)S(1)}, u32[]{:S(2)}, u32[]{:S(2)}) collective-permute-start(bf16[1,512]{1,0:T(2,128)(2,1)S(1)} %get-tuple-element.7), channel_id=1, source_target_pairs={{0,4},{4,8},{8,12},{12,16},{16,20},{20,24},{24,28},{1,5},{5,9},{9,... | collective-permute-start | bytes 3080 | tf_op jit(solution)/shard_map/ppermute | solution.py:16
  188.4 142.8 %collective-permute-start.3 = (bf16[1,512]{1,0:T(2,128)(2,1)S(1)}, bf16[1,512]{1,0:T(2,128)(2,1)S(1)}, u32[]{:S(2)}, u32[]{:S(2)}) collective-permute-start(bf16[1,512]{1,0:T(2,128)(2,1)S(1)} %get-tuple-element.8), channel_id=1, source_target_pairs={{4,0},{8,4},{12,8},{16,12},{20,16},{24,20},{28,24},{5,1},{9,5},{13... | collective-permute-start | bytes 3080 | tf_op jit(solution)/shard_map/ppermute | solution.py:17
  331.2 35.8 %copy-start.1 = (bf16[512,512]{1,0:T(8,128)(2,1)S(1)}, bf16[512,512]{1,0:T(8,128)(2,1)}, u32[]{:S(2)}) copy-start(bf16[512,512]{1,0:T(8,128)(2,1)} %param.8) | copy-start | bytes 1572868
  337.6 54.2 %all-gather.17.cloned.1.call-start = ((), (), s32[]{:S(2)}) async-start(), calls=%async_computation.8 | async-start | bytes 2621440 | tf_op jit(solution)/shard_map/all_gather | solution.py:32
  369.0 76.7 %reduce-scatter.5.cloned.1.call-start = ((), (), s32[]{:S(2)}) async-start(), calls=%async_computation.9 | async-start | bytes 2621440 | tf_op jit(solution)/shard_map/reduce_scatter | solution.py:57
  393.8 3.7 copy-start.3
  393.8 4.1 copy-start.5
  399.2 4.7 %collective-permute-start.4 = (bf16[1,512]{1,0:T(2,128)(2,1)S(1)}, bf16[1,512]{1,0:T(2,128)(2,1)S(1)}, u32[]{:S(2)}, u32[]{:S(2)}) collective-permute-start(bf16[1,512]{1,0:T(2,128)(2,1)S(1)} %get-tuple-element.5), channel_id=1, source_target_pairs={{0,4},{4,8},{8,12},{12,16},{16,20},{20,24},{24,28},{1,5},{5,9},{9,... | collective-permute-start | bytes 3080 | tf_op jit(solution)/shard_map/ppermute | solution.py:16
  402.6 5.5 %collective-permute-start.5 = (bf16[1,512]{1,0:T(2,128)(2,1)S(1)}, bf16[1,512]{1,0:T(2,128)(2,1)S(1)}, u32[]{:S(2)}, u32[]{:S(2)}) collective-permute-start(bf16[1,512]{1,0:T(2,128)(2,1)S(1)} %get-tuple-element.6), channel_id=1, source_target_pairs={{4,0},{8,4},{12,8},{16,12},{20,16},{24,20},{28,24},{5,1},{9,5},{13... | collective-permute-start | bytes 3080 | tf_op jit(solution)/shard_map/ppermute | solution.py:17
  408.1 37.7 %copy-start = (bf16[512,512]{1,0:T(8,128)(2,1)S(1)}, bf16[512,512]{1,0:T(8,128)(2,1)}, u32[]{:S(2)}) copy-start(bf16[512,512]{1,0:T(8,128)(2,1)} %add_convert_fusion.1) | copy-start | bytes 1572868
Sparse Core Ops, SparseCore 0:
  8.9 25.2 all-gather.6
  36.4 72.7 all-gather.12
  111.4 71.2 all-gather.10
  184.8 71.2 all-gather.8
  258.0 73.1 all-gather.14
  337.7 29.3 reduce-scatter.2
  369.2 22.5 all-gather.16
  414.6 31.1 reduce-scatter.4
where the time goes:
time: 455 us
  waiting for transfers between devices  386 us (85%)
  matrix products  25.4 us (6%)
  starting transfers between devices  15.4 us (3%)
  between operations  13.6 us (3%)
  other arithmetic  10.3 us (2%)
    all_gather x1, waiting for transfers between devices, per_device(): gathered_out = lax.all_gather(out_proj, 'sp', axis=2, tiled=True)  75.1 us
    all_gather x1, waiting for transfers between devices, per_device(): lax.all_gather(value_proj, 'sp', axis=1, tiled=True)  72.9 us
    all_gather x1, waiting for transfers between devices, per_device(): lax.all_gather(input_gate, 'sp', axis=1, tiled=True)  68.9 us
    all_gather x1, waiting for transfers between devices, per_device(): lax.all_gather(gate_proj, 'sp', axis=1, tiled=True)  66.4 us
    reduce_scatter x2, waiting for transfers between devices, per_device(): lax.psum_scatter(partials.astype(jnp.bfloat16), 'tp', scatter_dimension=1...  60.7 us
    all_gather x2, waiting for transfers between devices, per_device(): full_rows = lax.all_gather(current, 'tp', axis=1, tiled=True)  32.6 us
    dot_general x2, matrix products, per_device(): jnp.dot(gated, gathered_out[layer_index], preferred_element_type=jnp.floa...  12.7 us
    ppermute x3, starting transfers between devices, with_halo(): before = lax.ppermute(last, axis, up)  11.2 us
  transfers between devices with their start and end apart: 14, of which 10 were waited for; matrix products, arithmetic and copies ran while one was open for 3% of the time, Pallas kernels for 0%

commit v1 on v0

--- a/solution.py
+++ b/solution.py
@@ -1,6 +1,10 @@
+import functools
+
 import jax
 import jax.numpy as jnp
 from jax import lax
+from jax.experimental import pallas as pl
+from jax.experimental.pallas import tpu as pltpu
 from jax.sharding import PartitionSpec as P
 
 epsilon = 1e-06
@@ -61,7 +65,383 @@
     return current
 
 
+MESH = pl.DeviceIdType.MESH
+
+
+def fused_kernel(S, T, L, stream_ref, docs_ref, gain_ref, gate_ref, input_ref, value_ref, taps_ref, outw_ref,
+                 result_ref, win, wout, xfull, normed, cbuf, mpad, edge, halo, docpad, dhalo, mprev, mnext,
+                 gated, pbuf, rbuf, own_sem, w_send, w_recv, ag_send, ag_recv, rs_send, rs_recv,
+                 h_send, h_recv, d_send, d_recv, x_sem):
+    s = lax.axis_index("sp")
+    t = lax.axis_index("tp")
+    Z = S // 2
+    z, y = s // 2, s % 2
+    rows, width = stream_ref.shape
+    depth = gate_ref.shape[1]
+    cols = taps_ref.shape[2]
+    ow = outw_ref.shape[2]
+    per = S // T
+    units = 4 * L
+    mate = z + 1 - 2 * (z % 2)
+    sources = (input_ref, value_ref, gate_ref)
+    sends = []
+
+    barrier = pltpu.get_barrier_semaphore()
+
+    def greet(sp_index, tp_index):
+        pl.semaphore_signal(barrier, inc=1, device_id=(sp_index, tp_index), device_id_type=MESH)
+
+    nxt, prv = lax.rem(s + 1, S), lax.rem(s + S - 1, S)
+    greet(2 * z + 1 - y, t)
+    greet(nxt, t)
+    greet(prv, t)
+    for k in range(1, T):
+        greet(s, lax.rem(t + k, T))
+
+    @pl.when(z > 0)
+    def _():
+        greet(s - 2, t)
+
+    @pl.when(z < Z - 1)
+    def _():
+        greet(s + 2, t)
+
+    def slot(u, shard):
+        layer, part = u // 4, u % 4
+        if part < 3:
+            return win.at[layer * 3 + part, pl.ds(pl.multiple_of(shard * depth, depth), depth)]
+        return wout.at[layer, shard]
+
+    def own_copy(u):
+        layer, part = u // 4, u % 4
+        source = outw_ref.at[layer] if part == 3 else sources[part].at[layer]
+        return pltpu.make_async_copy(source, slot(u, s), own_sem.at[u])
+
+    x_copy = pltpu.make_async_copy(stream_ref, xfull.at[0, t], x_sem)
+    x_copy.start()
+    for u in range(units):
+        own_copy(u).start()
+
+    pl.semaphore_wait(barrier, T + 2 + jnp.where(z > 0, 1, 0) + jnp.where(z < Z - 1, 1, 0))
+
+    def w_copy(u, shard, way):
+        target = (s + 2, s - 2, 2 * z + 1 - y)[way]
+        return pltpu.make_async_remote_copy(
+            src_ref=slot(u, shard), dst_ref=slot(u, shard),
+            send_sem=w_send.at[way, u, shard], recv_sem=w_recv.at[u, shard],
+            device_id=(target, t), device_id_type=MESH)
+
+    def send(cond, copy_of):
+        @pl.when(cond)
+        def _():
+            copy_of().start()
+        sends.append((cond, copy_of))
+
+    def arrived(u, shard):
+        w_copy(u, shard, 2).wait_recv()
+
+    def own(u):
+        own_copy(u).wait()
+        send(z < Z - 1, lambda: w_copy(u, s, 0))
+        send(z > 0, lambda: w_copy(u, s, 1))
+        send(z >= 0, lambda: w_copy(u, s, 2))
+
+    def forward(u):
+        if u >= units:
+            return
+        if u + 2 < units:
+            own(u + 2)
+        through_mate = u % 2 == 1 and Z % 2 == 0
+        other = 2 * z + 1 - y
+        if through_mate:
+            arrived(u, other)
+            send(z % 2 == 0, lambda: w_copy(u, other, 0))
+            send(z % 2 == 1, lambda: w_copy(u, other, 1))
+        for d in range(1, Z):
+            for sign in (-1, 1):
+                at = z + sign * d
+                exists = (at >= 0) if sign < 0 else (at < Z)
+                shard = 2 * at + y
+
+                @pl.when(exists)
+                def _():
+                    arrived(u, shard)
+
+                onward = (z < Z - 1) if sign < 0 else (z > 0)
+                send(jnp.logical_and(exists, onward), lambda shard=shard, sign=sign: w_copy(u, shard, 0 if sign < 0 else 1))
+                across = jnp.logical_and(exists, at != mate) if through_mate and d == 1 else exists
+                send(across, lambda shard=shard: w_copy(u, shard, 2))
+
+    def others(u, use):
+        through_mate = u % 2 == 1 and Z % 2 == 0
+
+        def step(e, carry):
+            at = z + (1 - 2 * (e % 2)) * ((e + 1) // 2)
+            shard = 2 * at + 1 - y
+            inside = jnp.logical_and(at >= 0, at < Z)
+            fresh = jnp.logical_and(inside, e > 0) if through_mate else inside
+
+            @pl.when(fresh)
+            def _():
+                arrived(u, shard)
+
+            if use is not None:
+                @pl.when(inside)
+                def _():
+                    use(shard)
+            return carry
+
+        lax.fori_loop(0, 2 * Z - 1, step, 0)
+
+    def ag_copy(layer, k):
+        return pltpu.make_async_remote_copy(
+            src_ref=xfull.at[layer, t], dst_ref=xfull.at[layer, t],
+            send_sem=ag_send.at[layer, k], recv_sem=ag_recv.at[layer, t],
+            device_id=(s, lax.rem(t + k, T)), device_id_type=MESH)
+
+    def ag_wait(layer):
+        for k in range(1, T):
+            q = lax.rem(t + k, T)
+            pltpu.make_async_remote_copy(
+                src_ref=xfull.at[layer, q], dst_ref=xfull.at[layer, q],
+                send_sem=ag_send.at[layer, k], recv_sem=ag_recv.at[layer, q],
+                device_id=(s, q), device_id_type=MESH).wait_recv()
+
+    def ag_start(layer):
+        for k in range(1, T):
+            ag_copy(layer, k).start()
+
+    def halo_copy(layer, side):
+        return pltpu.make_async_remote_copy(
+            src_ref=edge.at[layer, 1 - side], dst_ref=halo.at[layer, side],
+            send_sem=h_send.at[layer, side], recv_sem=h_recv.at[layer, side],
+            device_id=((nxt, prv)[side], t), device_id_type=MESH)
+
+    def doc_copy(side):
+        return pltpu.make_async_remote_copy(
+            src_ref=docs_ref.at[pl.ds((rows - 8, 0)[side], 8)], dst_ref=dhalo.at[side],
+            send_sem=d_send.at[side], recv_sem=d_recv.at[side],
+            device_id=((nxt, prv)[side], t), device_id_type=MESH)
+
+    x_copy.wait()
+    own(0)
+    ag_start(0)
+    own(1)
+    for side in range(2):
+        doc_copy(side).start()
+
+    tile = rows // 2
+    small = rows // 8
+
+    def norm(layer):
+        def step(r, carry):
+            at = pl.ds(pl.multiple_of(r * small, small), small)
+            total = jnp.zeros((small, 1), jnp.float32)
+            for q in range(T):
+                wide = xfull[layer, q, at, :].astype(jnp.float32)
+                total = total + jnp.sum(wide * wide, axis=-1, keepdims=True)
+            scale = lax.rsqrt(total / (width * T) + epsilon)
+            for q in range(T):
+                wide = xfull[layer, q, at, :].astype(jnp.float32)
+                gain = gain_ref[layer:layer + 1, q * width:(q + 1) * width]
+                normed[at, q * width:(q + 1) * width] = (wide * scale * gain).astype(jnp.bfloat16)
+            return carry
+
+        lax.fori_loop(0, rows // small, step, 0)
+
+    def project(layer, part, use):
+        def step(r, carry):
+            start = pl.multiple_of(r * tile, tile)
+            at = pl.ds(start, tile)
+            product = jnp.dot(normed[at, :], win[layer * 3 + part], preferred_element_type=jnp.float32)
+            use(at, start, product.astype(jnp.bfloat16))
+            return carry
+
+        lax.fori_loop(0, rows // tile, step, 0)
+
+    def keep_gate(at, start, value):
+        cbuf[at, :] = value
+
+    def mix(at, start, value):
+        mixed = (cbuf[at, :].astype(jnp.float32) * value.astype(jnp.float32)).astype(jnp.bfloat16)
+        mpad[pl.ds(start + 8, tile), :] = mixed.astype(jnp.float32)
+
+    def masks():
+        for side in range(2):
+            doc_copy(side).wait_recv()
+        docpad[8:8 + rows, :] = docs_ref[...]
+        docpad[7:8, :] = jnp.where(s > 0, dhalo[0, 7:8, :], -1)
+        docpad[8 + rows:9 + rows, :] = jnp.where(s < S - 1, dhalo[1, 0:1, :], -1)
+        mprev[...] = jnp.where(docpad[7:7 + rows, :] == docs_ref[...], 1.0, 0.0)
+        mnext[...] = jnp.where(docpad[9:9 + rows, :] == docs_ref[...], 1.0, 0.0)
+
+    def convolve(layer):
+        for side in range(2):
+            halo_copy(layer, side).wait_recv()
+        mpad[7:8, :] = halo[layer, 0, 15:16, :].astype(jnp.float32)
+        mpad[8 + rows:9 + rows, :] = halo[layer, 1, 0:1, :].astype(jnp.float32)
+        for low in range(0, cols, 128):
+            lanes = slice(low, low + 128)
+            for r in range(0, rows, small):
+                before = taps_ref[layer, 0:1, lanes] * mpad[r + 7:r + 7 + small, lanes]
+                middle = taps_ref[layer, 1:2, lanes] * mpad[r + 8:r + 8 + small, lanes]
+                after = taps_ref[layer, 2:3, lanes] * mpad[r + 9:r + 9 + small, lanes]
+                here = slice(r, r + small)
+                total = (jnp.where(mprev[here, :] > 0.5, before, 0.0) + middle
+                         + jnp.where(mnext[here, :] > 0.5, after, 0.0))
+                gated[here, lanes] = (cbuf[here, lanes].astype(jnp.float32) * total).astype(jnp.bfloat16)
+
+    def rs_copy(layer, shard):
+        return pltpu.make_async_remote_copy(
+            src_ref=pbuf.at[layer, shard], dst_ref=rbuf.at[layer, t, shard % per],
+            send_sem=rs_send.at[layer, shard], recv_sem=rs_recv.at[layer, t, shard % per],
+            device_id=(s, shard // per), device_id_type=MESH)
+
+    def out_block(layer, shard):
+        part = jnp.dot(gated[...], wout[layer, shard], preferred_element_type=jnp.float32)
+        pbuf[layer, shard] = part.astype(jnp.bfloat16)
+
+        @pl.when(shard // per != t)
+        def _():
+            rs_copy(layer, shard).start()
+
+    def finish(layer):
+        for i in range(per):
+            for k in range(1, T):
+                q = lax.rem(t + k, T)
+                pltpu.make_async_remote_copy(
+                    src_ref=rbuf.at[layer, q, i], dst_ref=rbuf.at[layer, q, i],
+                    send_sem=rs_send.at[layer, i], recv_sem=rs_recv.at[layer, q, i],
+                    device_id=(s, q), device_id_type=MESH).wait_recv()
+
+        def step(r, carry):
+            at = pl.ds(pl.multiple_of(r * small, small), small)
+            for i in range(per):
+                lanes = slice(i * ow, (i + 1) * ow)
+                total = pbuf[layer, t * per + i, at, :].astype(jnp.float32)
+                for k in range(1, T):
+                    total = total + rbuf[layer, lax.rem(t + k, T), i, at, :].astype(jnp.float32)
+                fresh = (xfull[layer, t, at, lanes].astype(jnp.float32) + total).astype(jnp.bfloat16)
+                if layer + 1 < L:
+                    xfull[layer + 1, t, at, lanes] = fresh
+                else:
+                    result_ref[at, lanes] = fresh
+            return carry
+
+        lax.fori_loop(0, rows // small, step, 0)
+
+    forward(0)
+    forward(1)
+    for layer in range(L):
+        base = 4 * layer
+        forward(base + 2)
+        ag_wait(layer)
+        norm(layer)
+        others(base, None)
+        project(layer, 0, keep_gate)
+        others(base + 1, None)
+        project(layer, 1, mix)
+        edge[layer, 0] = mpad[8:24, :].astype(jnp.bfloat16)
+        edge[layer, 1] = mpad[rows - 8:rows + 8, :].astype(jnp.bfloat16)
+        for side in range(2):
+            halo_copy(layer, side).start()
+        if layer == 0:
+            masks()
+        forward(base + 3)
+        others(base + 2, None)
+        project(layer, 2, keep_gate)
+        convolve(layer)
+        forward(base + 4)
+
+        def column(at, carry):
+            out_block(layer, 2 * at + y)
+            return carry
+
+        lax.fori_loop(0, Z, column, 0)
+        others(base + 3, functools.partial(out_block, layer))
+        forward(base + 5)
+        finish(layer)
+        if layer + 1 < L:
+            ag_start(layer + 1)
+
+    for cond, copy_of in sends:
+        @pl.when(cond)
+        def _():
+            copy_of().wait_send()
+    for layer in range(L):
+        for k in range(1, T):
+            ag_copy(layer, k).wait_send()
+        for side in range(2):
+            halo_copy(layer, side).wait_send()
+
+        def drain(shard, carry):
+            @pl.when(shard // per != t)
+            def _():
+                rs_copy(layer, shard).wait_send()
+            return carry
+
+        lax.fori_loop(0, S, drain, 0)
+    for side in range(2):
+        doc_copy(side).wait_send()
+
+
+def fused(S, T, stream, doc_ids, norm_gain, gate_proj, input_gate, value_proj, taps, out_proj):
+    rows, width = stream.shape
+    L, depth, cols = gate_proj.shape
+    ow = out_proj.shape[2]
+    bf, f32, i32 = jnp.bfloat16, jnp.float32, jnp.int32
+    docs = jnp.broadcast_to(doc_ids[:, None], (rows, 128))
+    vmem, hbm = pl.BlockSpec(memory_space=pltpu.VMEM), pl.BlockSpec(memory_space=pl.ANY)
+    dma = pltpu.SemaphoreType.DMA
+    scratch = [
+        pltpu.VMEM((3 * L, S * depth, cols), bf),
+        pltpu.VMEM((L, S, cols, ow), bf),
+        pltpu.VMEM((L, T, rows, width), bf),
+        pltpu.VMEM((rows, T * width), bf),
+        pltpu.VMEM((rows, cols), bf),
+        pltpu.VMEM((rows + 16, cols), f32),
+        pltpu.VMEM((L, 2, 16, cols), bf),
+        pltpu.VMEM((L, 2, 16, cols), bf),
+        pltpu.VMEM((rows + 16, 128), i32),
+        pltpu.VMEM((2, 8, 128), i32),
+        pltpu.VMEM((rows, 128), f32),
+        pltpu.VMEM((rows, 128), f32),
+        pltpu.VMEM((rows, cols), bf),
+        pltpu.VMEM((L, S, rows, ow), bf),
+        pltpu.VMEM((L, T, S // T, rows, ow), bf),
+        dma((4 * L,)),
+        dma((3, 4 * L, S)),
+        dma((4 * L, S)),
+        dma((L, T)),
+        dma((L, T)),
+        dma((L, S)),
+        dma((L, T, S // T)),
+        dma((L, 2)),
+        dma((L, 2)),
+        dma((2,)),
+        dma((2,)),
+        dma,
+    ]
+    return pl.pallas_call(
+        functools.partial(fused_kernel, S, T, L),
+        out_shape=jax.ShapeDtypeStruct((rows, width), bf),
+        in_specs=[hbm, vmem, vmem, hbm, hbm, hbm, vmem, hbm],
+        out_specs=vmem,
+        scratch_shapes=scratch,
+        compiler_params=pltpu.CompilerParams(
+            collective_id=0, has_side_effects=True, vmem_limit_bytes=60 * 1024 * 1024),
+    )(stream, docs, norm_gain, gate_proj, input_gate, value_proj, taps, out_proj)
+
+
 def solution(mesh):
+    sp, tp = mesh.shape["sp"], mesh.shape["tp"]
+
+    def body(*arrays):
+        out_width = arrays[7].shape[2]
+        if out_width % 128 == 0 and sp % 2 == 0 and sp % tp == 0:
+            return fused(sp, tp, *arrays)
+        return per_device(*arrays)
+
     in_specs = (
         P("sp", "tp"),
         P("sp"),
@@ -74,5 +454,5 @@
     )
     out_specs = P("sp", "tp")
     return jax.shard_map(
-        per_device, mesh=mesh, in_specs=in_specs, out_specs=out_specs, check_vma=False
+        body, mesh=mesh, in_specs=in_specs, out_specs=out_specs, check_vma=False
     )

time: 455 us -> 202 us (0.44)
  waiting for transfers between devices: 386 us -> 0 us
  Pallas kernels: 0 us -> 195 us
  matrix products: 25.4 us -> 0 us
  starting transfers between devices: 15.4 us -> 0 us
  between operations: 13.6 us -> 0.01 us
  other arithmetic: 10.3 us -> 0 us
    all_gather x6 -> x0, waiting for transfers between devices: 316 us -> none  [the longest x1 75.1 us: per_device(): gathered_out = lax.all_gather(out_proj, 'sp', axis=2, tiled=True)]
    pallas_call x0 -> x1, Pallas kernels: none -> 195 us  [fused(): pl.pallas_call(functools.partial(fused_kernel, S, T, L), out_shape=jax.Sh...]
    reduce_scatter x2 -> x0, waiting for transfers between devices: 60.7 us -> none  [per_device(): lax.psum_scatter(partials.astype(jnp.bfloat16), 'tp', scatter_dimension=1...]
    dot_general x6 -> x0, matrix products: 25.4 us -> none  [the longest x2 12.7 us: per_device(): jnp.dot(gated, gathered_out[layer_index], preferred_element_type=jnp.floa...]
    ppermute x6 -> x0, starting transfers between devices: 15.1 us -> none  [the longest x3 11.2 us: with_halo(): before = lax.ppermute(last, axis, up)]
    ppermute x6 -> x0, waiting for transfers between devices: 6.71 us -> none  [the longest x3 6.71 us: with_halo(): after = lax.ppermute(leading, axis, down)]
  transfers between devices with their start and end apart: 14 -> 0, of which waited for: 10 -> 0; matrix products, arithmetic and copies ran while one was open for 3% -> 0% of each run, Pallas kernels for 0% -> 0%
where the time goes in v1:
time: 202 us; the launch traced here: 199 us
  Pallas kernels  195 us (97%)
  local copies, waits for them, and re-layouts  4.03 us (2%)
    pallas_call x1, Pallas kernels, fused(): pl.pallas_call(functools.partial(fused_kernel, S, T, L), out_shape=jax.Sh...  195 us

profile of v1, /device:TPU:0, one launch (start us, length us, event | category | flops | bytes accessed | tf_op | source)
XLA Modules:
  0.0 199.3 jit_solution(10341610082417381960)
XLA Ops:
  0.0 0.0 copy-start
  0.0 1.3 copy.9.taps_ref
  1.3 0.0 copy-done
  1.3 0.8 broadcast_in_dim.2.docs_ref
  2.2 195.3 %shard_map.82 = bf16[512,512]{1,0:T(8,128)(2,1)} custom-call(bf16[512,512]{1,0:T(8,128)(2,1)} %stream_ref.1, s32[512,128]{1,0:T(8,128)} %broadcast_in_dim.2.docs_ref, f32[2,2048]{1,0:T(2,128)} %gain_ref.1, bf16[2,256,512]{2,1,0:T(8,128)(2,1)} %gate_ref.1, bf16[2,256,512]{2,1,0:T(8,128)(2,1)} %input_ref.1, bf16[2,256,512]{2,1,0:T(8,128)(2,1)} %value_ref.1, ...), custom_call_target="tpu_custom_call" | custom-call | tf_op jit(solution)/shard_map/pallas_call | solution.py:425
  197.4 1.9 copy.11
Async XLA Ops:
  0.0 1.3 copy-start

commit v2 on v1

--- a/solution.py
+++ b/solution.py
@@ -70,7 +70,7 @@
 
 def fused_kernel(S, T, L, stream_ref, docs_ref, gain_ref, gate_ref, input_ref, value_ref, taps_ref, outw_ref,
                  result_ref, win, wout, xfull, normed, cbuf, mpad, edge, halo, docpad, dhalo, mprev, mnext,
-                 gated, pbuf, rbuf, own_sem, w_send, w_recv, ag_send, ag_recv, rs_send, rs_recv,
+                 gated, pbuf, rbuf, own_sem, w_send, w_recv, ag_send, ag_recv, rs_send, rs_recv, sbuf, p_send, p_recv,
                  h_send, h_recv, d_send, d_recv, x_sem):
     s = lax.axis_index("sp")
     t = lax.axis_index("tp")
@@ -82,6 +82,8 @@
     ow = outw_ref.shape[2]
     per = S // T
     units = 4 * L
+    sibling = t + 1 - 2 * (t % 2)
+    adders = [sibling] + [lax.rem(t + k, T) for k in range(2, T, 2)]
     mate = z + 1 - 2 * (z % 2)
     sources = (input_ref, value_ref, gate_ref)
     sends = []
@@ -146,31 +148,35 @@
         send(z > 0, lambda: w_copy(u, s, 1))
         send(z >= 0, lambda: w_copy(u, s, 2))
 
-    def forward(u):
+    def forward(u, whole=True):
         if u >= units:
             return
-        if u + 2 < units:
-            own(u + 2)
+        if u + 1 < units:
+            own(u + 1)
         through_mate = u % 2 == 1 and Z % 2 == 0
         other = 2 * z + 1 - y
         if through_mate:
             arrived(u, other)
             send(z % 2 == 0, lambda: w_copy(u, other, 0))
             send(z % 2 == 1, lambda: w_copy(u, other, 1))
-        for d in range(1, Z):
-            for sign in (-1, 1):
-                at = z + sign * d
-                exists = (at >= 0) if sign < 0 else (at < Z)
-                shard = 2 * at + y
-
-                @pl.when(exists)
-                def _():
-                    arrived(u, shard)
-
-                onward = (z < Z - 1) if sign < 0 else (z > 0)
-                send(jnp.logical_and(exists, onward), lambda shard=shard, sign=sign: w_copy(u, shard, 0 if sign < 0 else 1))
-                across = jnp.logical_and(exists, at != mate) if through_mate and d == 1 else exists
-                send(across, lambda shard=shard: w_copy(u, shard, 2))
+        for d in range(1, Z if whole else 2):
+            onward_step(u, d)
+
+    def onward_step(u, d):
+        through_mate = u % 2 == 1 and Z % 2 == 0
+        for sign in (-1, 1):
+            at = z + sign * d
+            exists = (at >= 0) if sign < 0 else (at < Z)
+            shard = 2 * at + y
+
+            @pl.when(exists)
+            def _():
+                arrived(u, shard)
+
+            onward = (z < Z - 1) if sign < 0 else (z > 0)
+            send(jnp.logical_and(exists, onward), lambda shard=shard, sign=sign: w_copy(u, shard, 0 if sign < 0 else 1))
+            across = jnp.logical_and(exists, at != mate) if through_mate and d == 1 else exists
+            send(across, lambda shard=shard: w_copy(u, shard, 2))
 
     def others(u, use):
         through_mate = u % 2 == 1 and Z % 2 == 0
@@ -226,7 +232,6 @@
     x_copy.wait()
     own(0)
     ag_start(0)
-    own(1)
     for side in range(2):
         doc_copy(side).start()
 
@@ -283,9 +288,9 @@
         for low in range(0, cols, 128):
             lanes = slice(low, low + 128)
             for r in range(0, rows, small):
-                before = taps_ref[layer, 0:1, lanes] * mpad[r + 7:r + 7 + small, lanes]
-                middle = taps_ref[layer, 1:2, lanes] * mpad[r + 8:r + 8 + small, lanes]
-                after = taps_ref[layer, 2:3, lanes] * mpad[r + 9:r + 9 + small, lanes]
+                before = taps_ref[0, layer:layer + 1, lanes] * mpad[r + 7:r + 7 + small, lanes]
+                middle = taps_ref[1, layer:layer + 1, lanes] * mpad[r + 8:r + 8 + small, lanes]
+                after = taps_ref[2, layer:layer + 1, lanes] * mpad[r + 9:r + 9 + small, lanes]
                 here = slice(r, r + small)
                 total = (jnp.where(mprev[here, :] > 0.5, before, 0.0) + middle
                          + jnp.where(mnext[here, :] > 0.5, after, 0.0))
@@ -297,18 +302,36 @@
             send_sem=rs_send.at[layer, shard], recv_sem=rs_recv.at[layer, t, shard % per],
             device_id=(s, shard // per), device_id_type=MESH)
 
+    def pair_copy(layer, shard):
+        return pltpu.make_async_remote_copy(
+            src_ref=pbuf.at[layer, shard], dst_ref=sbuf.at[layer, shard],
+            send_sem=p_send.at[layer, shard], recv_sem=p_recv.at[layer, shard],
+            device_id=(s, sibling), device_id_type=MESH)
+
     def out_block(layer, shard):
         part = jnp.dot(gated[...], wout[layer, shard], preferred_element_type=jnp.float32)
         pbuf[layer, shard] = part.astype(jnp.bfloat16)
 
-        @pl.when(shard // per != t)
+        owner = shard // per
+        near, same = owner // 2 == t // 2, owner % 2 == t % 2
+
+        @pl.when(jnp.logical_and(jnp.logical_not(near), jnp.logical_not(same)))
+        def _():
+            pair_copy(layer, shard).start()
+
+        @pl.when(jnp.logical_and(jnp.logical_not(near), same))
+        def _():
+            pair_copy(layer, shard).wait_recv()
+            both = part + sbuf[layer, shard].astype(jnp.float32)
+            pbuf[layer, shard] = both.astype(jnp.bfloat16)
+
+        @pl.when(near != same)
         def _():
             rs_copy(layer, shard).start()
 
     def finish(layer):
         for i in range(per):
-            for k in range(1, T):
-                q = lax.rem(t + k, T)
+            for q in adders:
                 pltpu.make_async_remote_copy(
                     src_ref=rbuf.at[layer, q, i], dst_ref=rbuf.at[layer, q, i],
                     send_sem=rs_send.at[layer, i], recv_sem=rs_recv.at[layer, q, i],
@@ -319,8 +342,8 @@
             for i in range(per):
                 lanes = slice(i * ow, (i + 1) * ow)
                 total = pbuf[layer, t * per + i, at, :].astype(jnp.float32)
-                for k in range(1, T):
-                    total = total + rbuf[layer, lax.rem(t + k, T), i, at, :].astype(jnp.float32)
+                for q in adders:
+                    total = total + rbuf[layer, q, i, at, :].astype(jnp.float32)
                 fresh = (xfull[layer, t, at, lanes].astype(jnp.float32) + total).astype(jnp.bfloat16)
                 if layer + 1 < L:
                     xfull[layer + 1, t, at, lanes] = fresh
@@ -347,17 +370,28 @@
             halo_copy(layer, side).start()
         if layer == 0:
             masks()
-        forward(base + 3)
+        last = layer == L - 1
+        forward(base + 3, whole=not last)
         others(base + 2, None)
         project(layer, 2, keep_gate)
         convolve(layer)
         forward(base + 4)
 
-        def column(at, carry):
-            out_block(layer, 2 * at + y)
+        def column(e, carry):
+            at = z + (1 - 2 * (e % 2)) * ((e + 1) // 2)
+
+            @pl.when(jnp.logical_and(at >= 0, at < Z))
+            def _():
+                out_block(layer, 2 * at + y)
             return carry
 
-        lax.fori_loop(0, Z, column, 0)
+        if last:
+            lax.fori_loop(0, min(3, 2 * Z - 1), column, 0)
+            for d in range(2, Z):
+                onward_step(base + 3, d)
+                lax.fori_loop(2 * d - 1, 2 * d + 1, column, 0)
+        else:
+            lax.fori_loop(0, 2 * Z - 1, column, 0)
         others(base + 3, functools.partial(out_block, layer))
         forward(base + 5)
         finish(layer)
@@ -375,9 +409,16 @@
             halo_copy(layer, side).wait_send()
 
         def drain(shard, carry):
-            @pl.when(shard // per != t)
+            owner = shard // per
+            near, same = owner // 2 == t // 2, owner % 2 == t % 2
+
+            @pl.when(near != same)
             def _():
                 rs_copy(layer, shard).wait_send()
+
+            @pl.when(jnp.logical_and(jnp.logical_not(near), jnp.logical_not(same)))
+            def _():
+                pair_copy(layer, shard).wait_send()
             return carry
 
         lax.fori_loop(0, S, drain, 0)
@@ -416,6 +457,9 @@
         dma((L, T)),
         dma((L, S)),
         dma((L, T, S // T)),
+        pltpu.VMEM((L, S, rows, ow), bf),
+        dma((L, S)),
+        dma((L, S)),
         dma((L, 2)),
         dma((L, 2)),
         dma((2,)),
@@ -430,7 +474,7 @@
         scratch_shapes=scratch,
         compiler_params=pltpu.CompilerParams(
             collective_id=0, has_side_effects=True, vmem_limit_bytes=60 * 1024 * 1024),
-    )(stream, docs, norm_gain, gate_proj, input_gate, value_proj, taps, out_proj)
+    )(stream, docs, norm_gain, gate_proj, input_gate, value_proj, jnp.transpose(taps, (1, 0, 2)), out_proj)
 
 
 def solution(mesh):
@@ -438,7 +482,7 @@
 
     def body(*arrays):
         out_width = arrays[7].shape[2]
-        if out_width % 128 == 0 and sp % 2 == 0 and sp % tp == 0:
+        if out_width % 128 == 0 and sp % 2 == 0 and tp % 2 == 0 and sp % tp == 0:
             return fused(sp, tp, *arrays)
         return per_device(*arrays)
 

time: 202 us -> 191 us (0.946)
  Pallas kernels: 195 us -> 185 us
    pallas_call x1, Pallas kernels: 195 us -> 185 us  [fused(): pl.pallas_call(functools.partial(fused_kernel, S, T, L), out_shape=jax.Sh...]
where the time goes in v2:
time: 191 us; the launch traced here: 189 us
  Pallas kernels  185 us (97%)
  local copies, waits for them, and re-layouts  3.39 us (2%)
    pallas_call x1, Pallas kernels, fused(): pl.pallas_call(functools.partial(fused_kernel, S, T, L), out_shape=jax.Sh...  185 us

profile of v2, /device:TPU:0, one launch (start us, length us, event | category | flops | bytes accessed | tf_op | source)
XLA Modules:
  0.0 188.7 jit_solution(4985986911130988603)
XLA Ops:
  0.0 1.5 broadcast_in_dim.2.docs_ref
  1.5 185.3 %shard_map.82 = bf16[512,512]{1,0:T(8,128)(2,1)} custom-call(bf16[512,512]{1,0:T(8,128)(2,1)} %stream_ref.1, s32[512,128]{1,0:T(8,128)} %broadcast_in_dim.2.docs_ref, f32[2,2048]{1,0:T(2,128)} %gain_ref.1, bf16[2,256,512]{2,1,0:T(8,128)(2,1)} %gate_ref.1, bf16[2,256,512]{2,1,0:T(8,128)(2,1)} %input_ref.1, bf16[2,256,512]{2,1,0:T(8,128)(2,1)} %value_ref.1, ...), custom_call_target="tpu_custom_call" | custom-call | tf_op jit(solution)/shard_map/pallas_call | solution.py:469
  186.8 1.9 copy.10
